TPU v7x, 32 devices: a whole 2x2x4 slice. The times are simulated.
32 devices in a mesh: grp: 2 (over y), sp: 4 (over z), tp: 4 (over x, core).
Axes of the slice: x: 2, y: 2, z: 4, core: 2. Of those that a mesh axis runs over, the one named last changes fastest.
Arguments:
- queries: bfloat16 [1024, 512], P(('grp', 'sp'), 'tp'), parts along dimension 0, may hold values from -6 to 6
- key_rows: bfloat16 [1024, 512], P(('grp', 'sp'), 'tp'), parts along dimension 0, may hold values from -6 to 6
- value_rows: bfloat16 [1024, 512], P(('grp', 'sp'), 'tp'), parts along dimension 0, may hold values from -16 to 16
- key_bias: bfloat16 [8, 1024], P('tp', ('grp', 'sp')), parts along dimension 1, may hold values from -20 to 0
- residual: bfloat16 [1024, 2048], P(('grp', 'sp')), parts along dimension 0, may hold values from -6 to 6
- out_weight: bfloat16 [512, 2048], P('tp'), may hold values from -0.25 to 0.25
- norm_gain: bfloat16 [2048], replicated, may hold values from 0.099609375 to 1.8984375
- gate_weight: bfloat16 [2048, 3072], P('sp', 'tp'), may hold values from -0.125 to 0.125
- up_weight: bfloat16 [2048, 3072], P('sp', 'tp'), may hold values from -0.125 to 0.125
- down_weight: bfloat16 [3072, 2048], P('tp', 'sp'), may hold values from -0.109375 to 0.109375
Outputs:
- layer_out: bfloat16 [1024, 2048], P(('grp', 'sp')), parts along dimension 0
There are 2 independent parts, one for each index of `grp`. A program takes and returns all parts, laid end to end along the dimension named above; an argument that names none is the same for every part. Nothing has to cross between parts.
All inputs are finite; a program needn't handle non-finite values.
Results may differ from a plain program's by a relative error of at most 0.014.
Values may be sent and summed in bfloat16 or wider, within the bound.
A program may use at most 64 MiB of HBM per device.

v0:
```python
import jax
import jax.numpy as jnp
from jax import lax
from jax.sharding import PartitionSpec as P

norm_eps = 1e-05


def from_behind(value, axis, steps):
    count = lax.axis_size(axis)
    initial, last = (max(0, -steps), min(count, count - steps))
    return lax.ppermute(value, axis, [(source, source + steps) for source in range(initial, last)])


def stick_block(carry, query_heads, key_block, value_block, bias_block, query_pos, key_start):
    accum, kept_log = carry
    key_count = key_block.shape[0]
    head_count = query_heads.shape[1]
    key_heads = key_block.reshape(key_count, head_count, -1)
    value_heads = value_block.reshape(key_count, head_count, -1)
    scale = key_heads.shape[2] ** (-0.5)
    scores = (
        jnp.einsum("qhd,khd->hqk", query_heads, key_heads, preferred_element_type=jnp.float32)
        * scale
    )
    scores = scores + bias_block.astype(jnp.float32)[:, None, :]
    key_pos = key_start + lax.iota(jnp.int32, key_count)
    strict = ((key_pos[None, :] < query_pos[:, None]) & (key_pos[None, :] >= 0))[None]
    log_retained = jnp.where(strict, jax.nn.log_sigmoid(-scores), 0.0)
    between = lax.cumsum(log_retained, axis=2, reverse=True) - log_retained + kept_log[:, :, None]
    stick = jnp.where(strict, jnp.exp(jax.nn.log_sigmoid(scores) + between), 0.0).astype(
        jnp.bfloat16
    )
    accum = accum + jnp.einsum(
        "hqk,khd->qhd", stick, value_heads, preferred_element_type=jnp.float32
    )
    return (accum, kept_log + jnp.sum(log_retained, axis=2))


def normalize(middle_wide, norm_gain):
    mean_square = jnp.mean(middle_wide * middle_wide, axis=1, keepdims=True)
    return (middle_wide * lax.rsqrt(mean_square + norm_eps) * norm_gain.astype(jnp.float32)).astype(
        jnp.bfloat16
    )


def body(
    queries,
    key_rows,
    value_rows,
    key_bias,
    residual,
    out_weight,
    norm_gain,
    gate_weight,
    up_weight,
    down_weight,
):
    seg_rows = queries.shape[0]
    head_count = key_bias.shape[0]
    head_width = queries.shape[1] // head_count
    sp_count = lax.axis_size("sp")
    token_place = lax.axis_index("sp")
    query_heads = queries.reshape(seg_rows, head_count, head_width)
    query_pos = token_place * seg_rows + lax.iota(jnp.int32, seg_rows)
    start_carry = (
        jnp.zeros((seg_rows, head_count, head_width), jnp.float32),
        jnp.zeros((head_count, seg_rows), jnp.float32),
    )
    carry = stick_block(
        start_carry, query_heads, key_rows, value_rows, key_bias, query_pos, token_place * seg_rows
    )

    def advance(hop_index, state):
        carry_now, blocks = state
        blocks = from_behind((blocks[0], blocks[1], blocks[2]), "sp", 1)

        def attend(current):
            return stick_block(
                current,
                query_heads,
                blocks[0],
                blocks[1],
                blocks[2],
                query_pos,
                (token_place - hop_index) * seg_rows,
            )

        carry_now = lax.cond(token_place >= hop_index, attend, lambda current: current, carry_now)
        return (carry_now, blocks)

    carry, passed_blocks = lax.fori_loop(
        1, sp_count, advance, (carry, (key_rows, value_rows, key_bias))
    )
    attended = carry[0].reshape(seg_rows, head_count * head_width).astype(jnp.bfloat16)
    own_rows = seg_rows // lax.axis_size("tp")
    own_start = lax.axis_index("tp") * own_rows
    mixed = lax.psum_scatter(
        jnp.dot(attended, out_weight, preferred_element_type=jnp.float32).astype(jnp.bfloat16),
        "tp",
        scatter_dimension=0,
        tiled=True,
    ).astype(jnp.float32)
    own_residual = lax.dynamic_slice_in_dim(residual, own_start, own_rows, 0)
    middle = (own_residual.astype(jnp.float32) + mixed).astype(jnp.bfloat16)
    middle_wide = middle.astype(jnp.float32)
    normed_all = lax.all_gather(normalize(middle_wide, norm_gain), "tp", axis=0, tiled=True)
    gate_pre = jnp.dot(
        normed_all,
        lax.all_gather(gate_weight, "sp", axis=0, tiled=True),
        preferred_element_type=jnp.float32,
    )
    up_pre = jnp.dot(
        normed_all,
        lax.all_gather(up_weight, "sp", axis=0, tiled=True),
        preferred_element_type=jnp.float32,
    )
    hidden = (jax.nn.silu(gate_pre) * up_pre).astype(jnp.bfloat16)
    down_terms = jnp.dot(
        hidden,
        lax.all_gather(down_weight, "sp", axis=1, tiled=True),
        preferred_element_type=jnp.float32,
    )
    down_sum = lax.psum_scatter(
        down_terms.astype(jnp.bfloat16), "tp", scatter_dimension=0, tiled=True
    ).astype(jnp.float32)
    own_out = (middle_wide + down_sum).astype(jnp.bfloat16)
    return lax.all_gather(own_out, "tp", axis=0, tiled=True)


def solution(mesh):
    in_specs = (
        P(("grp", "sp"), "tp"),
        P(("grp", "sp"), "tp"),
        P(("grp", "sp"), "tp"),
        P("tp", ("grp", "sp")),
        P(("grp", "sp"), None),
        P("tp", None),
        P(),
        P("sp", "tp"),
        P("sp", "tp"),
        P("tp", "sp"),
    )
    out_specs = P(("grp", "sp"), None)
    return jax.shard_map(body, mesh=mesh, in_specs=in_specs, out_specs=out_specs, check_vma=False)
```

profile of v0, /device:TPU:0, one launch (start us, length us, event | category | flops | bytes accessed | tf_op | source)
XLA Modules:
  0.0 288.5 jit_solution(2027559084728312409)
XLA Ops:
  11.2 2.2 reduce_window_sum.16
  13.7 38.2 %while.22 = (s32[]{:T(128)}, f32[128,2,64]{0,2,1:T(8,128)S(1)}, f32[2,128]{1,0:T(2,128)S(1)}, bf16[128,128]{0,1:T(8,128)(2,1)S(1)}, bf16[128,128]{0,1:T(8,128)(2...) while((s32[]{:T(128)}, f32[128,2,64]{0,2,1:T(8,128)S(1)}, ...), condition=%wide.region_7.8_spmd.clone, body=%wide.region_2.7_spmd.clone.sunk | while | flops 13992710 | bytes 1652875 | solution.py:92
  13.7 5.0 %collective-permute-start = (bf16[128,128]{0,1:T(8,128)(2,1)S(1)}, bf16[128,128]{0,1:T(8,128)(2,1)S(1)}, u32[]{:S(2)}, u32[]{:S(2)}) collective-permute-start(bf16[128,128]{0,1:T(8,128)(2,1)S(1)} %get-tuple-element.347), channel_id=1, source_target_pairs={{0,4},{4,8},{8,12},{1,5},{5,9},{9,13},{2,6},{6,10},{10,14},{3,7},{... | collective-permute-start | bytes 98312 | tf_op jit(solution)/shard_map/while/body/eval_jaxpr/ppermute | solution.py:12
  18.7 3.5 %collective-permute-start.2 = (bf16[128,128]{0,1:T(8,128)(2,1)S(1)}, bf16[128,128]{0,1:T(8,128)(2,1)S(1)}, u32[]{:S(2)}, u32[]{:S(2)}) collective-permute-start(bf16[128,128]{0,1:T(8,128)(2,1)S(1)} %get-tuple-element.348), channel_id=1, source_target_pairs={{0,4},{4,8},{8,12},{1,5},{5,9},{9,13},{2,6},{6,10},{10,14},{3,7},{... | collective-permute-start | bytes 98312 | tf_op jit(solution)/shard_map/while/body/eval_jaxpr/ppermute | solution.py:12
  22.2 3.5 %collective-permute-start.1 = (bf16[2,128]{1,0:T(2,128)(2,1)S(1)}, bf16[2,128]{1,0:T(2,128)(2,1)S(1)}, u32[]{:S(2)}, u32[]{:S(2)}) collective-permute-start(bf16[2,128]{1,0:T(2,128)(2,1)S(1)} %get-tuple-element.349), channel_id=1, source_target_pairs={{0,4},{4,8},{8,12},{1,5},{5,9},{9,13},{2,6},{6,10},{10,14},{3,7},{... | collective-permute-start | bytes 1544 | tf_op jit(solution)/shard_map/while/body/eval_jaxpr/ppermute | solution.py:12
  25.7 1.3 collective-permute-done.1
  27.0 7.2 %collective-permute-start = (bf16[128,128]{0,1:T(8,128)(2,1)S(1)}, bf16[128,128]{0,1:T(8,128)(2,1)S(1)}, u32[]{:S(2)}, u32[]{:S(2)}) collective-permute-start(bf16[128,128]{0,1:T(8,128)(2,1)S(1)} %get-tuple-element.347), channel_id=1, source_target_pairs={{0,4},{4,8},{8,12},{1,5},{5,9},{9,13},{2,6},{6,10},{10,14},{3,7},{... | collective-permute-start | bytes 98312 | tf_op jit(solution)/shard_map/while/body/eval_jaxpr/ppermute | solution.py:12
  34.3 1.9 collective-permute-start.2
  36.2 1.9 collective-permute-start.1
  38.2 1.3 collective-permute-done.1
  39.5 4.2 %collective-permute-start = (bf16[128,128]{0,1:T(8,128)(2,1)S(1)}, bf16[128,128]{0,1:T(8,128)(2,1)S(1)}, u32[]{:S(2)}, u32[]{:S(2)}) collective-permute-start(bf16[128,128]{0,1:T(8,128)(2,1)S(1)} %get-tuple-element.347), channel_id=1, source_target_pairs={{0,4},{4,8},{8,12},{1,5},{5,9},{9,13},{2,6},{6,10},{10,14},{3,7},{... | collective-permute-start | bytes 98312 | tf_op jit(solution)/shard_map/while/body/eval_jaxpr/ppermute | solution.py:12
  43.7 5.0 %collective-permute-start.2 = (bf16[128,128]{0,1:T(8,128)(2,1)S(1)}, bf16[128,128]{0,1:T(8,128)(2,1)S(1)}, u32[]{:S(2)}, u32[]{:S(2)}) collective-permute-start(bf16[128,128]{0,1:T(8,128)(2,1)S(1)} %get-tuple-element.348), channel_id=1, source_target_pairs={{0,4},{4,8},{8,12},{1,5},{5,9},{9,13},{2,6},{6,10},{10,14},{3,7},{... | collective-permute-start | bytes 98312 | tf_op jit(solution)/shard_map/while/body/eval_jaxpr/ppermute | solution.py:12
  48.7 1.9 collective-permute-start.1
  50.6 1.3 collective-permute-done.1
  55.0 21.9 %reduce-scatter.3.cloned.1.call-done = bf16[32,2048]{1,0:T(8,128)(2,1)} async-done(((bf16[128,2048]{1,0:T(8,128)(2,1)}), bf16[32,2048]{1,0:T(8,128)(2,1)}) %reduce-scatter.3.cloned.1.call-update) | async-done | bytes 131088 | tf_op jit(solution)/shard_map/reduce_scatter | solution.py:98
  76.9 1.1 fusion.21
  78.1 6.6 %all_gather.15 = bf16[128,2048]{1,0:T(8,128)(2,1)S(1)} all-gather(bf16[32,2048]{1,0:T(8,128)(2,1)S(1)} %fusion.23), channel_id=1, replica_groups=mesh['grp'=2,'sp'=4,'tp'=4] {'tp'}, dimensions={0}, use_global_device_ids=true | all-gather | bytes 655360 | tf_op jit(solution)/shard_map/all_gather | solution.py:107
  84.7 35.7 %all-gather.4.cloned.1.call-done = bf16[2048,768]{1,0:T(8,128)(2,1)} async-done(((bf16[512,768]{1,0:T(8,128)(2,1)}), bf16[2048,768]{1,0:T(8,128)(2,1)}) %all-gather.4.cloned.1.call-update) | async-done | bytes 3145744 | tf_op jit(solution)/shard_map/all_gather | solution.py:110
  120.4 2.5 fusion.37
  122.9 60.9 %all-gather.6.cloned.1.call-done = bf16[2048,768]{1,0:T(8,128)(2,1)} async-done(((bf16[512,768]{1,0:T(8,128)(2,1)}), bf16[2048,768]{1,0:T(8,128)(2,1)}) %all-gather.6.cloned.1.call-update) | async-done | bytes 3145744 | tf_op jit(solution)/shard_map/all_gather | solution.py:115
  183.8 63.4 %all-gather.8.cloned.1.call-done = bf16[768,2048]{1,0:T(8,128)(2,1)} async-done(((bf16[768,512]{1,0:T(8,128)(2,1)}), bf16[768,2048]{1,0:T(8,128)(2,1)}) %all-gather.8.cloned.1.call-update) | async-done | bytes 3145744 | tf_op jit(solution)/shard_map/all_gather | solution.py:121
  247.3 4.9 %convolution_convert_fusion = bf16[128,2048]{1,0:T(8,128)(2,1)} fusion(bf16[768,2048]{1,0:T(8,128)(2,1)} %all-gather.8.cloned.1.call-done, bf16[128,2048]{1,0:T(8,128)(2,1)S(1)} %all_gather.15, bf16[2048,768]{1,0:T(8,128)(2,1)} %all-gather.6.cloned.1.call-done, f32[128,768]{1,0:T(8,128)S(1)} %fusion.37), kind=kOutput, calls=%fused_computation.22 | convolution fusion | flops 806158336 | bytes 7733248 | tf_op jit(solution)/shard_map/dot_general | solution.py:119
  252.2 20.4 %reduce-scatter.5.cloned.1.call-done = bf16[32,2048]{1,0:T(8,128)(2,1)} async-done(((bf16[128,2048]{1,0:T(8,128)(2,1)}), bf16[32,2048]{1,0:T(8,128)(2,1)}) %reduce-scatter.5.cloned.1.call-update) | async-done | bytes 131088 | tf_op jit(solution)/shard_map/reduce_scatter | solution.py:124
  273.6 6.6 %all_gather.19 = bf16[128,2048]{1,0:T(8,128)(2,1)S(1)} all-gather(bf16[32,2048]{1,0:T(8,128)(2,1)S(1)} %fusion.24), channel_id=1, replica_groups=mesh['grp'=2,'sp'=4,'tp'=4] {'tp'}, dimensions={0}, use_global_device_ids=true | all-gather | bytes 655360 | tf_op jit(solution)/shard_map/all_gather | solution.py:128
  (53 shorter events, 9.0 us)
Async XLA Ops:
  7.4 44.6 %copy-start = (bf16[128,2048]{1,0:T(8,128)(2,1)S(1)}, bf16[128,2048]{1,0:T(8,128)(2,1)}, u32[]{:S(2)}) copy-start(bf16[128,2048]{1,0:T(8,128)(2,1)} %param.19) | copy-start | bytes 1572868
  7.4 69.5 %reduce-scatter.3.cloned.1.call-start = ((), (), s32[]{:S(2)}) async-start(), calls=%async_computation.2 | async-start | bytes 655360 | tf_op jit(solution)/shard_map/reduce_scatter | solution.py:98
  13.7 13.2 %collective-permute-start = (bf16[128,128]{0,1:T(8,128)(2,1)S(1)}, bf16[128,128]{0,1:T(8,128)(2,1)S(1)}, u32[]{:S(2)}, u32[]{:S(2)}) collective-permute-start(bf16[128,128]{0,1:T(8,128)(2,1)S(1)} %get-tuple-element.347), channel_id=1, source_target_pairs={{0,4},{4,8},{8,12},{1,5},{5,9},{9,13},{2,6},{6,10},{10,14},{3,7},{... | collective-permute-start | bytes 98312 | tf_op jit(solution)/shard_map/while/body/eval_jaxpr/ppermute | solution.py:12
  18.7 8.3 %collective-permute-start.2 = (bf16[128,128]{0,1:T(8,128)(2,1)S(1)}, bf16[128,128]{0,1:T(8,128)(2,1)S(1)}, u32[]{:S(2)}, u32[]{:S(2)}) collective-permute-start(bf16[128,128]{0,1:T(8,128)(2,1)S(1)} %get-tuple-element.348), channel_id=1, source_target_pairs={{0,4},{4,8},{8,12},{1,5},{5,9},{9,13},{2,6},{6,10},{10,14},{3,7},{... | collective-permute-start | bytes 98312 | tf_op jit(solution)/shard_map/while/body/eval_jaxpr/ppermute | solution.py:12
  22.2 4.8 %collective-permute-start.1 = (bf16[2,128]{1,0:T(2,128)(2,1)S(1)}, bf16[2,128]{1,0:T(2,128)(2,1)S(1)}, u32[]{:S(2)}, u32[]{:S(2)}) collective-permute-start(bf16[2,128]{1,0:T(2,128)(2,1)S(1)} %get-tuple-element.349), channel_id=1, source_target_pairs={{0,4},{4,8},{8,12},{1,5},{5,9},{9,13},{2,6},{6,10},{10,14},{3,7},{... | collective-permute-start | bytes 1544 | tf_op jit(solution)/shard_map/while/body/eval_jaxpr/ppermute | solution.py:12
  27.0 12.4 %collective-permute-start = (bf16[128,128]{0,1:T(8,128)(2,1)S(1)}, bf16[128,128]{0,1:T(8,128)(2,1)S(1)}, u32[]{:S(2)}, u32[]{:S(2)}) collective-permute-start(bf16[128,128]{0,1:T(8,128)(2,1)S(1)} %get-tuple-element.347), channel_id=1, source_target_pairs={{0,4},{4,8},{8,12},{1,5},{5,9},{9,13},{2,6},{6,10},{10,14},{3,7},{... | collective-permute-start | bytes 98312 | tf_op jit(solution)/shard_map/while/body/eval_jaxpr/ppermute | solution.py:12
  34.3 5.1 %collective-permute-start.2 = (bf16[128,128]{0,1:T(8,128)(2,1)S(1)}, bf16[128,128]{0,1:T(8,128)(2,1)S(1)}, u32[]{:S(2)}, u32[]{:S(2)}) collective-permute-start(bf16[128,128]{0,1:T(8,128)(2,1)S(1)} %get-tuple-element.348), channel_id=1, source_target_pairs={{0,4},{4,8},{8,12},{1,5},{5,9},{9,13},{2,6},{6,10},{10,14},{3,7},{... | collective-permute-start | bytes 98312 | tf_op jit(solution)/shard_map/while/body/eval_jaxpr/ppermute | solution.py:12
  36.2 3.2 %collective-permute-start.1 = (bf16[2,128]{1,0:T(2,128)(2,1)S(1)}, bf16[2,128]{1,0:T(2,128)(2,1)S(1)}, u32[]{:S(2)}, u32[]{:S(2)}) collective-permute-start(bf16[2,128]{1,0:T(2,128)(2,1)S(1)} %get-tuple-element.349), channel_id=1, source_target_pairs={{0,4},{4,8},{8,12},{1,5},{5,9},{9,13},{2,6},{6,10},{10,14},{3,7},{... | collective-permute-start | bytes 1544 | tf_op jit(solution)/shard_map/while/body/eval_jaxpr/ppermute | solution.py:12
  39.5 12.4 %collective-permute-start = (bf16[128,128]{0,1:T(8,128)(2,1)S(1)}, bf16[128,128]{0,1:T(8,128)(2,1)S(1)}, u32[]{:S(2)}, u32[]{:S(2)}) collective-permute-start(bf16[128,128]{0,1:T(8,128)(2,1)S(1)} %get-tuple-element.347), channel_id=1, source_target_pairs={{0,4},{4,8},{8,12},{1,5},{5,9},{9,13},{2,6},{6,10},{10,14},{3,7},{... | collective-permute-start | bytes 98312 | tf_op jit(solution)/shard_map/while/body/eval_jaxpr/ppermute | solution.py:12
  43.7 8.2 %collective-permute-start.2 = (bf16[128,128]{0,1:T(8,128)(2,1)S(1)}, bf16[128,128]{0,1:T(8,128)(2,1)S(1)}, u32[]{:S(2)}, u32[]{:S(2)}) collective-permute-start(bf16[128,128]{0,1:T(8,128)(2,1)S(1)} %get-tuple-element.348), channel_id=1, source_target_pairs={{0,4},{4,8},{8,12},{1,5},{5,9},{9,13},{2,6},{6,10},{10,14},{3,7},{... | collective-permute-start | bytes 98312 | tf_op jit(solution)/shard_map/while/body/eval_jaxpr/ppermute | solution.py:12
  48.7 3.2 %collective-permute-start.1 = (bf16[2,128]{1,0:T(2,128)(2,1)S(1)}, bf16[2,128]{1,0:T(2,128)(2,1)S(1)}, u32[]{:S(2)}, u32[]{:S(2)}) collective-permute-start(bf16[2,128]{1,0:T(2,128)(2,1)S(1)} %get-tuple-element.349), channel_id=1, source_target_pairs={{0,4},{4,8},{8,12},{1,5},{5,9},{9,13},{2,6},{6,10},{10,14},{3,7},{... | collective-permute-start | bytes 1544 | tf_op jit(solution)/shard_map/while/body/eval_jaxpr/ppermute | solution.py:12
  52.0 3.0 %copy-start.1 = (bf16[2048]{0:T(1024)(128)(2,1)S(1)}, bf16[2048]{0:T(1024)(128)(2,1)}, u32[]{:S(2)}) copy-start(bf16[2048]{0:T(1024)(128)(2,1)} %param.20) | copy-start | bytes 12292
  53.2 67.3 %all-gather.4.cloned.1.call-start = ((), (), s32[]{:S(2)}) async-start(), calls=%async_computation.3 | async-start | bytes 3932160 | tf_op jit(solution)/shard_map/all_gather | solution.py:110
  53.7 130.1 %all-gather.6.cloned.1.call-start = ((), (), s32[]{:S(2)}) async-start(), calls=%async_computation.4 | async-start | bytes 3932160 | tf_op jit(solution)/shard_map/all_gather | solution.py:115
  54.3 192.9 %all-gather.8.cloned.1.call-start = ((), (), s32[]{:S(2)}) async-start(), calls=%async_computation.5 | async-start | bytes 3932160 | tf_op jit(solution)/shard_map/all_gather | solution.py:121
  54.9 217.7 %reduce-scatter.5.cloned.1.call-start = ((), (), s32[]{:S(2)}) async-start(), calls=%async_computation.6 | async-start | bytes 655360 | tf_op jit(solution)/shard_map/reduce_scatter | solution.py:124
Sparse Core Ops, SparseCore 0:
  53.3 23.5 reduce-scatter.2
  252.3 20.2 reduce-scatter.4
Sparse Core Ops, SparseCore 1:
  55.2 65.2 all-gather.3
  121.9 61.9 all-gather.5
  185.3 61.9 all-gather.7
where the time goes:
time: 289 us
  waiting for transfers between devices  208 us (72%)
  starting transfers between devices  34.3 us (12%)
  between operations  15.1 us (5%)
  blocking collectives  13.2 us (5%)
  matrix products  9.04 us (3%)
  other arithmetic  4.64 us (2%)
  local copies, waits for them, and re-layouts  4.15 us (1%)
    all_gather x1, waiting for transfers between devices, body(): lax.all_gather(down_weight, 'sp', axis=1, tiled=True)  63.4 us
    all_gather x1, waiting for transfers between devices, body(): lax.all_gather(up_weight, 'sp', axis=0, tiled=True)  60.9 us
    all_gather x1, waiting for transfers between devices, body(): lax.all_gather(gate_weight, 'sp', axis=0, tiled=True)  35.7 us
    ppermute x9, starting transfers between devices, from_behind(): lax.ppermute(value, axis, [(source, source + steps) for source in range(i...  34.1 us
    reduce_scatter x1, waiting for transfers between devices, body(): lax.psum_scatter(jnp.dot(attended, out_weight, preferred_element_type=jnp...  21.9 us
    reduce_scatter x1, waiting for transfers between devices, body(): lax.psum_scatter(down_terms.astype(jnp.bfloat16), 'tp', scatter_dimension...  20.4 us
    all_gather x1, blocking collectives, body(): lax.all_gather(normalize(middle_wide, norm_gain), 'tp', axis=0, tiled=True)  6.6 us
    all_gather x1, blocking collectives, body(): return lax.all_gather(own_out, 'tp', axis=0, tiled=True)  6.58 us
  transfers between devices with their start and end apart: 14, of which 8 were waited for; matrix products, arithmetic and copies ran while one was open for 1% of the time, Pallas kernels for 0%

commit v1 on v0

--- a/solution.py
+++ b/solution.py
@@ -4,6 +4,11 @@
 from jax.sharding import PartitionSpec as P
 
 norm_eps = 1e-05
+
+
+def stack_and_merge(array, mesh_axis, along):
+    blocks = lax.all_gather(array, mesh_axis)
+    return jnp.concatenate(blocks, axis=along)
 
 
 def from_behind(value, axis, steps):
@@ -117,9 +122,7 @@
     )
     hidden = (jax.nn.silu(gate_pre) * up_pre).astype(jnp.bfloat16)
     down_terms = jnp.dot(
-        hidden,
-        lax.all_gather(down_weight, "sp", axis=1, tiled=True),
-        preferred_element_type=jnp.float32,
+        hidden, stack_and_merge(down_weight, "sp", 1), preferred_element_type=jnp.float32
     )
     down_sum = lax.psum_scatter(
         down_terms.astype(jnp.bfloat16), "tp", scatter_dimension=0, tiled=True

time: 289 us -> 290 us (level)
  waiting for transfers between devices: 208 us -> 203 us
  local copies, waits for them, and re-layouts: 4.15 us -> 8.8 us
    all_gather x1, waiting for transfers between devices: 63.4 us -> 35.7 us  [stack_and_merge(): blocks = lax.all_gather(array, mesh_axis)]
    all_gather x1, waiting for transfers between devices: 35.7 us -> 58.8 us  [body(): lax.all_gather(gate_weight, 'sp', axis=0, tiled=True)]
    reshape x0 -> x1, local copies, waits for them, and re-layouts: none -> 4.65 us  [stack_and_merge(): return jnp.concatenate(blocks, axis=along)]
  transfers between devices with their start and end apart: 14 -> 14, of which waited for: 8 -> 8; matrix products, arithmetic and copies ran while one was open for 1% -> 3% of each run, Pallas kernels for 0% -> 0%
where the time goes in v1:
time: 290 us; the launch traced here: 289 us
  waiting for transfers between devices  203 us (70%)
  starting transfers between devices  34.3 us (12%)
  between operations  15.1 us (5%)
  blocking collectives  13.2 us (5%)
  matrix products  9.43 us (3%)
  local copies, waits for them, and re-layouts  8.8 us (3%)
  other arithmetic  4.64 us (2%)
    all_gather x1, waiting for transfers between devices, body(): lax.all_gather(up_weight, 'sp', axis=0, tiled=True)  60.9 us
    all_gather x1, waiting for transfers between devices, body(): lax.all_gather(gate_weight, 'sp', axis=0, tiled=True)  58.8 us
    all_gather x1, waiting for transfers between devices, stack_and_merge(): blocks = lax.all_gather(array, mesh_axis)  35.7 us
    ppermute x9, starting transfers between devices, from_behind(): lax.ppermute(value, axis, [(source, source + steps) for source in range(i...  34.1 us
    reduce_scatter x1, waiting for transfers between devices, body(): lax.psum_scatter(jnp.dot(attended, out_weight, preferred_element_type=jnp...  21.9 us
    reduce_scatter x1, waiting for transfers between devices, body(): lax.psum_scatter(down_terms.astype(jnp.bfloat16), 'tp', scatter_dimension...  20.4 us
    all_gather x1, blocking collectives, body(): lax.all_gather(normalize(middle_wide, norm_gain), 'tp', axis=0, tiled=True)  6.6 us
    all_gather x1, blocking collectives, body(): return lax.all_gather(own_out, 'tp', axis=0, tiled=True)  6.58 us
  transfers between devices with their start and end apart: 14, of which 8 were waited for; matrix products, arithmetic and copies ran while one was open for 3% of the time, Pallas kernels for 0%

profile of v1, /device:TPU:0, one launch (start us, length us, event | category | flops | bytes accessed | tf_op | source)
XLA Modules:
  0.0 288.9 jit_solution(6189614997878790938)
XLA Ops:
  11.2 2.2 reduce_window_sum.16
  13.7 38.2 %while.22 = (s32[]{:T(128)}, f32[128,2,64]{0,2,1:T(8,128)S(1)}, f32[2,128]{1,0:T(2,128)S(1)}, bf16[128,128]{0,1:T(8,128)(2,1)S(1)}, bf16[128,128]{0,1:T(8,128)(2...) while((s32[]{:T(128)}, f32[128,2,64]{0,2,1:T(8,128)S(1)}, ...), condition=%wide.region_7.8_spmd.clone, body=%wide.region_2.7_spmd.clone.sunk | while | flops 13992710 | bytes 1652875 | solution.py:97
  13.7 5.0 %collective-permute-start = (bf16[128,128]{0,1:T(8,128)(2,1)S(1)}, bf16[128,128]{0,1:T(8,128)(2,1)S(1)}, u32[]{:S(2)}, u32[]{:S(2)}) collective-permute-start(bf16[128,128]{0,1:T(8,128)(2,1)S(1)} %get-tuple-element.356), channel_id=1, source_target_pairs={{0,4},{4,8},{8,12},{1,5},{5,9},{9,13},{2,6},{6,10},{10,14},{3,7},{... | collective-permute-start | bytes 98312 | tf_op jit(solution)/shard_map/while/body/eval_jaxpr/ppermute | solution.py:17
  18.7 3.5 %collective-permute-start.2 = (bf16[128,128]{0,1:T(8,128)(2,1)S(1)}, bf16[128,128]{0,1:T(8,128)(2,1)S(1)}, u32[]{:S(2)}, u32[]{:S(2)}) collective-permute-start(bf16[128,128]{0,1:T(8,128)(2,1)S(1)} %get-tuple-element.357), channel_id=1, source_target_pairs={{0,4},{4,8},{8,12},{1,5},{5,9},{9,13},{2,6},{6,10},{10,14},{3,7},{... | collective-permute-start | bytes 98312 | tf_op jit(solution)/shard_map/while/body/eval_jaxpr/ppermute | solution.py:17
  22.2 3.5 %collective-permute-start.1 = (bf16[2,128]{1,0:T(2,128)(2,1)S(1)}, bf16[2,128]{1,0:T(2,128)(2,1)S(1)}, u32[]{:S(2)}, u32[]{:S(2)}) collective-permute-start(bf16[2,128]{1,0:T(2,128)(2,1)S(1)} %get-tuple-element.358), channel_id=1, source_target_pairs={{0,4},{4,8},{8,12},{1,5},{5,9},{9,13},{2,6},{6,10},{10,14},{3,7},{... | collective-permute-start | bytes 1544 | tf_op jit(solution)/shard_map/while/body/eval_jaxpr/ppermute | solution.py:17
  25.7 1.3 collective-permute-done.1
  27.0 7.2 %collective-permute-start = (bf16[128,128]{0,1:T(8,128)(2,1)S(1)}, bf16[128,128]{0,1:T(8,128)(2,1)S(1)}, u32[]{:S(2)}, u32[]{:S(2)}) collective-permute-start(bf16[128,128]{0,1:T(8,128)(2,1)S(1)} %get-tuple-element.356), channel_id=1, source_target_pairs={{0,4},{4,8},{8,12},{1,5},{5,9},{9,13},{2,6},{6,10},{10,14},{3,7},{... | collective-permute-start | bytes 98312 | tf_op jit(solution)/shard_map/while/body/eval_jaxpr/ppermute | solution.py:17
  34.3 1.9 collective-permute-start.2
  36.2 1.9 collective-permute-start.1
  38.2 1.3 collective-permute-done.1
  39.5 4.2 %collective-permute-start = (bf16[128,128]{0,1:T(8,128)(2,1)S(1)}, bf16[128,128]{0,1:T(8,128)(2,1)S(1)}, u32[]{:S(2)}, u32[]{:S(2)}) collective-permute-start(bf16[128,128]{0,1:T(8,128)(2,1)S(1)} %get-tuple-element.356), channel_id=1, source_target_pairs={{0,4},{4,8},{8,12},{1,5},{5,9},{9,13},{2,6},{6,10},{10,14},{3,7},{... | collective-permute-start | bytes 98312 | tf_op jit(solution)/shard_map/while/body/eval_jaxpr/ppermute | solution.py:17
  43.7 5.0 %collective-permute-start.2 = (bf16[128,128]{0,1:T(8,128)(2,1)S(1)}, bf16[128,128]{0,1:T(8,128)(2,1)S(1)}, u32[]{:S(2)}, u32[]{:S(2)}) collective-permute-start(bf16[128,128]{0,1:T(8,128)(2,1)S(1)} %get-tuple-element.357), channel_id=1, source_target_pairs={{0,4},{4,8},{8,12},{1,5},{5,9},{9,13},{2,6},{6,10},{10,14},{3,7},{... | collective-permute-start | bytes 98312 | tf_op jit(solution)/shard_map/while/body/eval_jaxpr/ppermute | solution.py:17
  48.7 1.9 collective-permute-start.1
  50.6 1.3 collective-permute-done.1
  55.0 21.9 %reduce-scatter.3.cloned.1.call-done = bf16[32,2048]{1,0:T(8,128)(2,1)} async-done(((bf16[128,2048]{1,0:T(8,128)(2,1)}), bf16[32,2048]{1,0:T(8,128)(2,1)}) %reduce-scatter.3.cloned.1.call-update) | async-done | bytes 131088 | tf_op jit(solution)/shard_map/reduce_scatter | solution.py:103
  78.1 6.6 %all_gather.18 = bf16[128,2048]{1,0:T(8,128)(2,1)S(1)} all-gather(bf16[32,2048]{1,0:T(8,128)(2,1)S(1)} %fusion.23), channel_id=1, replica_groups=mesh['grp'=2,'sp'=4,'tp'=4] {'tp'}, dimensions={0}, use_global_device_ids=true | all-gather | bytes 655360 | tf_op jit(solution)/shard_map/all_gather | solution.py:112
  84.7 35.7 %all-gather.9.cloned.1.call-done = bf16[3072,512]{1,0:T(8,128)(2,1)} async-done(((bf16[768,512]{1,0:T(8,128)(2,1)}), bf16[3072,512]{1,0:T(8,128)(2,1)}) %all-gather.9.cloned.1.call-update) | async-done | bytes 3145744 | tf_op jit(solution)/shard_map/all_gather | solution.py:10
  120.4 4.7 %copy.32 = bf16[768,4,512]{0,2,1:T(8,128)(2,1)} copy(bf16[768,4,512]{2,0,1:T(8,128)(2,1)} %bitcast.30) | data formatting | bytes 6291456 | tf_op jit(solution)/shard_map/reshape | solution.py:11
  125.1 58.8 %all-gather.5.cloned.1.call-done = bf16[2048,768]{1,0:T(8,128)(2,1)} async-done(((bf16[512,768]{1,0:T(8,128)(2,1)}), bf16[2048,768]{1,0:T(8,128)(2,1)}) %all-gather.5.cloned.1.call-update) | async-done | bytes 3145744 | tf_op jit(solution)/shard_map/all_gather | solution.py:115
  183.8 2.5 fusion.37
  186.3 60.9 %all-gather.7.cloned.1.call-done = bf16[2048,768]{1,0:T(8,128)(2,1)} async-done(((bf16[512,768]{1,0:T(8,128)(2,1)}), bf16[2048,768]{1,0:T(8,128)(2,1)}) %all-gather.7.cloned.1.call-update) | async-done | bytes 3145744 | tf_op jit(solution)/shard_map/all_gather | solution.py:120
  247.3 5.3 %convolution_convert_fusion = bf16[128,2048]{1,0:T(8,128)(2,1)} fusion(bf16[768,2048]{0,1:T(8,128)(2,1)} %bitcast.31, bf16[128,2048]{1,0:T(8,128)(2,1)S(1)} %all_gather.18, bf16[2048,768]{1,0:T(8,128)(2,1)} %all-gather.7.cloned.1.call-done, f32[128,768]{1,0:T(8,128)S(1)} %fusion.37), kind=kOutput, calls=%fused_computation.22 | convolution fusion | flops 806158336 | bytes 7733248 | tf_op jit(solution)/shard_map/dot_general | solution.py:124
  252.6 20.4 %reduce-scatter.5.cloned.1.call-done = bf16[32,2048]{1,0:T(8,128)(2,1)} async-done(((bf16[128,2048]{1,0:T(8,128)(2,1)}), bf16[32,2048]{1,0:T(8,128)(2,1)}) %reduce-scatter.5.cloned.1.call-update) | async-done | bytes 131088 | tf_op jit(solution)/shard_map/reduce_scatter | solution.py:127
  274.0 6.6 %all_gather.23 = bf16[128,2048]{1,0:T(8,128)(2,1)S(1)} all-gather(bf16[32,2048]{1,0:T(8,128)(2,1)S(1)} %fusion.24), channel_id=1, replica_groups=mesh['grp'=2,'sp'=4,'tp'=4] {'tp'}, dimensions={0}, use_global_device_ids=true | all-gather | bytes 655360 | tf_op jit(solution)/shard_map/all_gather | solution.py:131
  (54 shorter events, 10.1 us)
Async XLA Ops:
  7.4 44.6 %copy-start = (bf16[128,2048]{1,0:T(8,128)(2,1)S(1)}, bf16[128,2048]{1,0:T(8,128)(2,1)}, u32[]{:S(2)}) copy-start(bf16[128,2048]{1,0:T(8,128)(2,1)} %param.19) | copy-start | bytes 1572868
  7.4 69.5 %reduce-scatter.3.cloned.1.call-start = ((), (), s32[]{:S(2)}) async-start(), calls=%async_computation.2 | async-start | bytes 655360 | tf_op jit(solution)/shard_map/reduce_scatter | solution.py:103
  13.7 13.2 %collective-permute-start = (bf16[128,128]{0,1:T(8,128)(2,1)S(1)}, bf16[128,128]{0,1:T(8,128)(2,1)S(1)}, u32[]{:S(2)}, u32[]{:S(2)}) collective-permute-start(bf16[128,128]{0,1:T(8,128)(2,1)S(1)} %get-tuple-element.356), channel_id=1, source_target_pairs={{0,4},{4,8},{8,12},{1,5},{5,9},{9,13},{2,6},{6,10},{10,14},{3,7},{... | collective-permute-start | bytes 98312 | tf_op jit(solution)/shard_map/while/body/eval_jaxpr/ppermute | solution.py:17
  18.7 8.3 %collective-permute-start.2 = (bf16[128,128]{0,1:T(8,128)(2,1)S(1)}, bf16[128,128]{0,1:T(8,128)(2,1)S(1)}, u32[]{:S(2)}, u32[]{:S(2)}) collective-permute-start(bf16[128,128]{0,1:T(8,128)(2,1)S(1)} %get-tuple-element.357), channel_id=1, source_target_pairs={{0,4},{4,8},{8,12},{1,5},{5,9},{9,13},{2,6},{6,10},{10,14},{3,7},{... | collective-permute-start | bytes 98312 | tf_op jit(solution)/shard_map/while/body/eval_jaxpr/ppermute | solution.py:17
  22.2 4.8 %collective-permute-start.1 = (bf16[2,128]{1,0:T(2,128)(2,1)S(1)}, bf16[2,128]{1,0:T(2,128)(2,1)S(1)}, u32[]{:S(2)}, u32[]{:S(2)}) collective-permute-start(bf16[2,128]{1,0:T(2,128)(2,1)S(1)} %get-tuple-element.358), channel_id=1, source_target_pairs={{0,4},{4,8},{8,12},{1,5},{5,9},{9,13},{2,6},{6,10},{10,14},{3,7},{... | collective-permute-start | bytes 1544 | tf_op jit(solution)/shard_map/while/body/eval_jaxpr/ppermute | solution.py:17
  27.0 12.4 %collective-permute-start = (bf16[128,128]{0,1:T(8,128)(2,1)S(1)}, bf16[128,128]{0,1:T(8,128)(2,1)S(1)}, u32[]{:S(2)}, u32[]{:S(2)}) collective-permute-start(bf16[128,128]{0,1:T(8,128)(2,1)S(1)} %get-tuple-element.356), channel_id=1, source_target_pairs={{0,4},{4,8},{8,12},{1,5},{5,9},{9,13},{2,6},{6,10},{10,14},{3,7},{... | collective-permute-start | bytes 98312 | tf_op jit(solution)/shard_map/while/body/eval_jaxpr/ppermute | solution.py:17
  34.3 5.1 %collective-permute-start.2 = (bf16[128,128]{0,1:T(8,128)(2,1)S(1)}, bf16[128,128]{0,1:T(8,128)(2,1)S(1)}, u32[]{:S(2)}, u32[]{:S(2)}) collective-permute-start(bf16[128,128]{0,1:T(8,128)(2,1)S(1)} %get-tuple-element.357), channel_id=1, source_target_pairs={{0,4},{4,8},{8,12},{1,5},{5,9},{9,13},{2,6},{6,10},{10,14},{3,7},{... | collective-permute-start | bytes 98312 | tf_op jit(solution)/shard_map/while/body/eval_jaxpr/ppermute | solution.py:17
  36.2 3.2 %collective-permute-start.1 = (bf16[2,128]{1,0:T(2,128)(2,1)S(1)}, bf16[2,128]{1,0:T(2,128)(2,1)S(1)}, u32[]{:S(2)}, u32[]{:S(2)}) collective-permute-start(bf16[2,128]{1,0:T(2,128)(2,1)S(1)} %get-tuple-element.358), channel_id=1, source_target_pairs={{0,4},{4,8},{8,12},{1,5},{5,9},{9,13},{2,6},{6,10},{10,14},{3,7},{... | collective-permute-start | bytes 1544 | tf_op jit(solution)/shard_map/while/body/eval_jaxpr/ppermute | solution.py:17
  39.5 12.4 %collective-permute-start = (bf16[128,128]{0,1:T(8,128)(2,1)S(1)}, bf16[128,128]{0,1:T(8,128)(2,1)S(1)}, u32[]{:S(2)}, u32[]{:S(2)}) collective-permute-start(bf16[128,128]{0,1:T(8,128)(2,1)S(1)} %get-tuple-element.356), channel_id=1, source_target_pairs={{0,4},{4,8},{8,12},{1,5},{5,9},{9,13},{2,6},{6,10},{10,14},{3,7},{... | collective-permute-start | bytes 98312 | tf_op jit(solution)/shard_map/while/body/eval_jaxpr/ppermute | solution.py:17
  43.7 8.2 %collective-permute-start.2 = (bf16[128,128]{0,1:T(8,128)(2,1)S(1)}, bf16[128,128]{0,1:T(8,128)(2,1)S(1)}, u32[]{:S(2)}, u32[]{:S(2)}) collective-permute-start(bf16[128,128]{0,1:T(8,128)(2,1)S(1)} %get-tuple-element.357), channel_id=1, source_target_pairs={{0,4},{4,8},{8,12},{1,5},{5,9},{9,13},{2,6},{6,10},{10,14},{3,7},{... | collective-permute-start | bytes 98312 | tf_op jit(solution)/shard_map/while/body/eval_jaxpr/ppermute | solution.py:17
  48.7 3.2 %collective-permute-start.1 = (bf16[2,128]{1,0:T(2,128)(2,1)S(1)}, bf16[2,128]{1,0:T(2,128)(2,1)S(1)}, u32[]{:S(2)}, u32[]{:S(2)}) collective-permute-start(bf16[2,128]{1,0:T(2,128)(2,1)S(1)} %get-tuple-element.358), channel_id=1, source_target_pairs={{0,4},{4,8},{8,12},{1,5},{5,9},{9,13},{2,6},{6,10},{10,14},{3,7},{... | collective-permute-start | bytes 1544 | tf_op jit(solution)/shard_map/while/body/eval_jaxpr/ppermute | solution.py:17
  52.0 3.0 %copy-start.1 = (bf16[2048]{0:T(1024)(128)(2,1)S(1)}, bf16[2048]{0:T(1024)(128)(2,1)}, u32[]{:S(2)}) copy-start(bf16[2048]{0:T(1024)(128)(2,1)} %param.20) | copy-start | bytes 12292
  53.2 67.3 %all-gather.9.cloned.1.call-start = ((), (), s32[]{:S(2)}) async-start(), calls=%async_computation.6 | async-start | bytes 3932160 | tf_op jit(solution)/shard_map/all_gather | solution.py:10
  53.7 130.1 %all-gather.5.cloned.1.call-start = ((), (), s32[]{:S(2)}) async-start(), calls=%async_computation.3 | async-start | bytes 3932160 | tf_op jit(solution)/shard_map/all_gather | solution.py:115
  54.3 192.9 %all-gather.7.cloned.1.call-start = ((), (), s32[]{:S(2)}) async-start(), calls=%async_computation.4 | async-start | bytes 3932160 | tf_op jit(solution)/shard_map/all_gather | solution.py:120
  54.9 218.1 %reduce-scatter.5.cloned.1.call-start = ((), (), s32[]{:S(2)}) async-start(), calls=%async_computation.5 | async-start | bytes 655360 | tf_op jit(solution)/shard_map/reduce_scatter | solution.py:127
Sparse Core Ops, SparseCore 0:
  53.3 23.5 reduce-scatter.2
  252.7 20.2 reduce-scatter.4
Sparse Core Ops, SparseCore 1:
  55.2 65.2 all-gather.8
  121.9 61.9 all-gather.4
  185.3 61.9 all-gather.6
